TPU v7x, 32 devices: a whole 2x2x4 slice. The times are simulated.
32 devices in a mesh: sp: 8 (over z, y), tp: 4 (over x, core).
Axes of the slice: x: 2, y: 2, z: 4, core: 2. Of those that a mesh axis runs over, the one named last changes fastest.
Arguments:
- queries: bfloat16 [1024, 1280], P('sp', 'tp'), may hold values from -4000 to 4000
- latents: bfloat16 [1024, 512], P('sp'), may hold values from -6 to 6
- shared_key: bfloat16 [1024, 64], P('sp'), may hold values from -4 to 4
- expand_weight: bfloat16 [512, 1536], P(None, 'tp'), may hold values from -0.25 to 0.25
- residual: bfloat16 [1024, 2048], P('sp'), may hold values from -3 to 3
- out_weight: bfloat16 [768, 2048], replicated, may hold values from -0.21875 to 0.21875
- norm_gain: bfloat16 [2048], replicated, may hold values from 0.099609375 to 1.8984375
- gate_weight: bfloat16 [2048, 3072], P('sp', 'tp'), may hold values from -0.125 to 0.125
- value_weight: bfloat16 [2048, 3072], P('sp', 'tp'), may hold values from -0.125 to 0.125
- conv_weight: bfloat16 [3, 3072], P(None, 'tp'), may hold values from -3.5 to 3.5
- down_weight: bfloat16 [3072, 2048], P('tp', 'sp'), may hold values from -0.109375 to 0.109375
Outputs:
- output: bfloat16 [1024, 2048], P(('sp', 'tp'))
All inputs are finite; a program needn't handle non-finite values.
Results may differ from a plain program's by a relative error of at most 0.018.
Values may be sent and summed in bfloat16 or wider, within the bound.
A program may use at most 128 MiB of HBM per device.

v0:
```python
import jax
import jax.numpy as jnp
from jax import lax
from jax.sharding import PartitionSpec as P

NOPE_A = 128
VAL_A = 128
NOPE_B = 64
VAL_B = 64
ROPE = 64


def padded_2(block, sides, width):
    for axis, dim in sides:
        count = lax.axis_size(axis)
        forward = [(i, i + 1) for i in range(count - 1)]
        backward = [(target, source) for source, target in forward]
        low = lax.ppermute(
            lax.slice_in_dim(block, block.shape[dim] - width, None, axis=dim), axis, forward
        )
        high = lax.ppermute(lax.slice_in_dim(block, 0, width, axis=dim), axis, backward)
        block = jnp.concatenate([low, block, high], axis=dim)
    return block


def tables(positions, width):
    half_width = width // 2
    frequency = 10000.0 ** (-jnp.arange(half_width, dtype=jnp.float32) / half_width)
    angles = positions.astype(jnp.float32)[:, None] * frequency[None, :]
    return (jnp.cos(angles), jnp.sin(angles))


def rotate(vectors, cos_table, sine_table):
    half_width = vectors.shape[-1] // 2
    first_half = vectors[:, :half_width].astype(jnp.float32)
    second_half = vectors[:, half_width:].astype(jnp.float32)
    turned = jnp.concatenate(
        [
            first_half * cos_table - second_half * sine_table,
            second_half * cos_table + first_half * sine_table,
        ],
        axis=1,
    )
    return turned.astype(jnp.bfloat16)


def normalize(stream, norm_gain):
    stream_f = stream.astype(jnp.float32)
    scaled = stream_f * lax.rsqrt(jnp.mean(stream_f * stream_f, axis=1, keepdims=True) + 1e-06)
    return (scaled * norm_gain.astype(jnp.float32)).astype(jnp.bfloat16)


def update(running, q_content, q_turned, k_content, k_turned, values, score_scale):
    row_max, row_sum, weighted = running
    scores = (
        jnp.einsum("qd,kd->qk", q_content, k_content, preferred_element_type=jnp.float32)
        + jnp.einsum("qd,kd->qk", q_turned, k_turned, preferred_element_type=jnp.float32)
    ) * score_scale
    new_max = jnp.maximum(row_max, jnp.max(scores, axis=1))
    weights = jnp.exp(scores - new_max[:, None])
    row_sum = jnp.sum(weights, axis=1)
    weighted = jnp.dot(weights.astype(jnp.bfloat16), values, preferred_element_type=jnp.float32)
    return (new_max, row_sum, weighted)


def body(
    queries,
    latents,
    shared_key,
    expand_weight,
    residual,
    out_weight,
    norm_gain,
    gate_weight,
    value_weight,
    conv_weight,
    down_weight,
):
    tok_rows = queries.shape[0]
    q_width = NOPE_A + NOPE_B + 2 * ROPE
    kv_width = NOPE_A + VAL_A + NOPE_B + VAL_B
    positions = lax.axis_index("sp") * tok_rows + jnp.arange(tok_rows, dtype=jnp.int32)
    cos_table, sine_table = tables(positions, ROPE)
    key_turned = rotate(shared_key, cos_table, sine_table)
    scale_wide = (NOPE_A + ROPE) ** (-0.5)
    scale_narrow = (NOPE_B + ROPE) ** (-0.5)
    initial = []
    pair_index = 0
    q_base = pair_index * q_width
    rotary_base = q_base + NOPE_A + NOPE_B
    wide_content = queries[:, q_base : q_base + NOPE_A]
    narrow_content = queries[:, q_base + NOPE_A : rotary_base]
    wide_turned = rotate(queries[:, rotary_base : rotary_base + ROPE], cos_table, sine_table)
    narrow_turned = rotate(
        queries[:, rotary_base + ROPE : rotary_base + 2 * ROPE], cos_table, sine_table
    )
    query_parts = [(wide_content, wide_turned, narrow_content, narrow_turned)]
    lowest = jnp.full((tok_rows,), -1e30, jnp.float32)
    empty_sum = jnp.zeros((tok_rows,), jnp.float32)
    initial += [
        lowest,
        empty_sum,
        jnp.zeros((tok_rows, VAL_A), jnp.float32),
        lowest,
        empty_sum,
        jnp.zeros((tok_rows, VAL_B), jnp.float32),
    ]
    initial = tuple(initial)
    pieces = (
        lax.all_gather(latents, "sp", axis=0, tiled=True),
        lax.all_gather(key_turned, "sp", axis=0, tiled=True),
    )
    expanded = jnp.dot(pieces[0], expand_weight, preferred_element_type=jnp.float32).astype(
        jnp.bfloat16
    )
    turned_keys = pieces[1]
    result = []
    pair_index = 0
    wide_content, wide_turned, narrow_content, narrow_turned = query_parts[pair_index]
    kv_base = pair_index * kv_width
    narrow_base = kv_base + NOPE_A + VAL_A
    wide_keys = expanded[:, kv_base : kv_base + NOPE_A]
    wide_values = expanded[:, kv_base + NOPE_A : narrow_base]
    narrow_keys = expanded[:, narrow_base : narrow_base + NOPE_B]
    narrow_values = expanded[:, narrow_base + NOPE_B : narrow_base + NOPE_B + VAL_B]
    absorb_offset = 6 * pair_index
    result += list(
        update(
            initial[absorb_offset : absorb_offset + 3],
            wide_content,
            wide_turned,
            wide_keys,
            turned_keys,
            wide_values,
            scale_wide,
        )
    )
    result += list(
        update(
            initial[absorb_offset + 3 : absorb_offset + 6],
            narrow_content,
            narrow_turned,
            narrow_keys,
            turned_keys,
            narrow_values,
            scale_narrow,
        )
    )
    running = tuple(result)
    outputs = []
    pair_index = 0
    for group_index in range(2):
        offset = 6 * pair_index + 3 * group_index
        outputs.append((running[offset + 2] / running[offset + 1][:, None]).astype(jnp.bfloat16))
    attended = jnp.concatenate(outputs, axis=1)
    share = tok_rows // lax.axis_size("tp")
    tp_index = lax.axis_index("tp")
    all_heads = lax.all_gather(attended, "tp", axis=1, tiled=True)
    projected = jnp.dot(all_heads, out_weight, preferred_element_type=jnp.float32)
    stream = (residual.astype(jnp.float32) + projected).astype(jnp.bfloat16)
    normed = normalize(stream, norm_gain)
    stream_own = lax.dynamic_slice_in_dim(stream, tp_index * share, share, 0)
    pieces = (
        lax.all_gather(gate_weight, "sp", axis=0, tiled=True),
        lax.all_gather(value_weight, "sp", axis=0, tiled=True),
    )
    gate_sum = jnp.dot(normed, pieces[0], preferred_element_type=jnp.float32)
    value_sum = jnp.dot(normed, pieces[1], preferred_element_type=jnp.float32)
    gate_pre = gate_sum.astype(jnp.bfloat16)
    value_pre = value_sum.astype(jnp.bfloat16)
    reach = conv_weight.shape[0] // 2
    padded = padded_2(gate_pre, (("sp", 0),), reach)
    mixed_gate = jnp.zeros(gate_pre.shape, jnp.float32)
    for tap in range(conv_weight.shape[0]):
        mixed_gate = mixed_gate + padded[tap : tap + tok_rows].astype(jnp.float32) * conv_weight[
            tap
        ].astype(jnp.float32)
    active = (jax.nn.silu(mixed_gate) * value_pre.astype(jnp.float32)).astype(jnp.bfloat16)
    partial_rows = jnp.dot(
        active,
        lax.all_gather(down_weight, "sp", axis=1, tiled=True),
        preferred_element_type=jnp.float32,
    )
    summed = lax.psum_scatter(
        partial_rows.astype(jnp.bfloat16), "tp", scatter_dimension=0, tiled=True
    ).astype(jnp.float32)
    return (stream_own.astype(jnp.float32) + summed).astype(jnp.bfloat16)


def solution(mesh):
    in_specs = (
        P("sp", "tp"),
        P("sp", None),
        P("sp", None),
        P(None, "tp"),
        P("sp", None),
        P(),
        P(),
        P("sp", "tp"),
        P("sp", "tp"),
        P(None, "tp"),
        P("tp", "sp"),
    )
    out_specs = P(("sp", "tp"), None)
    return jax.shard_map(body, mesh=mesh, in_specs=in_specs, out_specs=out_specs, check_vma=False)
```

profile of v0, /device:TPU:0, one launch (start us, length us, event | category | flops | bytes accessed | tf_op | source)
XLA Modules:
  0.0 271.1 jit_solution(13108688686888295058)
XLA Ops:
  6.5 0.7 all-gather.5.cloned.1.call-update
  7.3 0.0 all-gather.7.cloned.1.call-start
  7.3 0.7 all-gather.7.cloned.1.call-update
  8.0 0.0 all-gather.11.cloned.1.call-start
  8.1 0.7 all-gather.11.cloned.1.call-update
  8.7 0.0 all-gather.9.cloned.1.call-start
  8.8 0.5 all-gather.9.cloned.1.call-update
  9.3 0.0 reduce-scatter.2.cloned.1.call-start
  9.4 0.7 convert_element_type.113
  10.1 0.9 fusion.59
  11.0 28.2 %all_gather.19 = bf16[1024,64]{0,1:T(8,128)(2,1)S(1)} all-gather(bf16[128,64]{0,1:T(8,128)(2,1)S(1)} %pad_maximum_fusion.5), channel_id=1, replica_groups=mesh['sp'=8,'tp'=4] {'sp'}, dimensions={0}, use_global_device_ids=true | all-gather | bytes 147456 | tf_op jit(solution)/shard_map/all_gather | solution.py:111
  39.2 13.5 %all-gather.5.cloned.1.call-done = bf16[1024,512]{1,0:T(8,128)(2,1)} async-done(((bf16[128,512]{1,0:T(8,128)(2,1)}), bf16[1024,512]{1,0:T(8,128)(2,1)}) %all-gather.5.cloned.1.call-update) | async-done | bytes 1048592 | tf_op jit(solution)/shard_map/all_gather | solution.py:110
  52.7 1.9 convolution_convert_fusion.1
  54.7 0.3 convolution_bitcast_fusion.1
  54.9 0.4 fusion.83
  55.3 0.2 fusion.11
  55.5 0.3 convolution_bitcast_fusion
  55.7 0.4 fusion.82
  56.1 0.2 fusion.13
  56.3 0.2 fusion.7
  56.5 0.3 fusion.6
  56.8 5.6 %all_gather.20 = bf16[128,768]{0,1:T(8,128)(2,1)S(1)} all-gather(bf16[128,192]{0,1:T(8,128)(2,1)S(1)} %pad_maximum_fusion.4), channel_id=1, replica_groups=mesh['sp'=8,'tp'=4] {'tp'}, dimensions={1}, use_global_device_ids=true | all-gather | bytes 245760 | tf_op jit(solution)/shard_map/all_gather | solution.py:158
  62.4 1.4 fusion.8
  63.8 49.9 %all-gather.7.cloned.1.call-done = bf16[2048,768]{1,0:T(8,128)(2,1)} async-done(((bf16[256,768]{1,0:T(8,128)(2,1)}), bf16[2048,768]{1,0:T(8,128)(2,1)}) %all-gather.7.cloned.1.call-update) | async-done | bytes 3145744 | tf_op jit(solution)/shard_map/all_gather | solution.py:164
  113.7 2.7 convolution_convert_fusion.3
  116.4 2.5 collective-permute-start
  118.8 1.3 collective-permute-start.1
  120.2 56.9 %all-gather.11.cloned.1.call-done = bf16[768,2048]{1,0:T(8,128)(2,1)} async-done(((bf16[768,256]{1,0:T(8,128)(2,1)}), bf16[768,2048]{1,0:T(8,128)(2,1)}) %all-gather.11.cloned.1.call-update) | async-done | bytes 3145744 | tf_op jit(solution)/shard_map/all_gather | solution.py:181
  177.1 60.3 %all-gather.9.cloned.1.call-done = bf16[2048,768]{1,0:T(8,128)(2,1)} async-done(((bf16[256,768]{1,0:T(8,128)(2,1)}), bf16[2048,768]{1,0:T(8,128)(2,1)}) %all-gather.9.cloned.1.call-update) | async-done | bytes 3145744 | tf_op jit(solution)/shard_map/all_gather | solution.py:165
  237.3 5.1 %convolution_convert_fusion = bf16[128,2048]{1,0:T(8,128)(2,1)} fusion(bf16[768,2048]{1,0:T(8,128)(2,1)} %all-gather.11.cloned.1.call-done, bf16[2048,768]{1,0:T(8,128)(2,1)} %all-gather.9.cloned.1.call-done, bf16[128,768]{1,0:T(8,128)(2,1)S(1)} %convolution_convert_fusion.3, bf16[1,768]{1,0:T(2,128)(2,1)S(1)} %collective-permute-done.1, ...), kind=kOutput, calls=%fused_computation.2 | convolution fusion | flops 808779776 | bytes 7557632 | tf_op jit(solution)/shard_map/dot_general | solution.py:179
  242.5 20.5 %reduce-scatter.2.cloned.1.call-done = bf16[32,2048]{1,0:T(8,128)(2,1)} async-done(((bf16[128,2048]{1,0:T(8,128)(2,1)}), bf16[32,2048]{1,0:T(8,128)(2,1)}) %reduce-scatter.2.cloned.1.call-update) | async-done | bytes 131088 | tf_op jit(solution)/shard_map/reduce_scatter | solution.py:184
  262.9 1.7 add_convert_fusion
  (21 shorter events, 0.1 us)
Async XLA Ops:
  6.5 55.8 %copy-start = (bf16[768,2048]{1,0:T(8,128)(2,1)S(1)}, bf16[768,2048]{1,0:T(8,128)(2,1)}, u32[]{:S(2)}) copy-start(bf16[768,2048]{1,0:T(8,128)(2,1)} %param.16) | copy-start | bytes 9437188
  6.5 48.1 %copy-start.2 = (bf16[128,320]{0,1:T(8,128)(2,1)S(1)}, bf16[128,320]{0,1:T(8,128)(2,1)}, u32[]{:S(2)}) copy-start(bf16[128,320]{0,1:T(8,128)(2,1)} %param.11) | copy-start | bytes 245764
  6.5 46.2 %all-gather.5.cloned.1.call-start = ((), (), s32[]{:S(2)}) async-start(), calls=%async_computation.1 | async-start | bytes 1179648 | tf_op jit(solution)/shard_map/all_gather | solution.py:110
  7.3 106.4 %all-gather.7.cloned.1.call-start = ((), (), s32[]{:S(2)}) async-start(), calls=%async_computation.2 | async-start | bytes 3538944 | tf_op jit(solution)/shard_map/all_gather | solution.py:164
  8.0 169.1 %all-gather.11.cloned.1.call-start = ((), (), s32[]{:S(2)}) async-start(), calls=%async_computation.4 | async-start | bytes 3538944 | tf_op jit(solution)/shard_map/all_gather | solution.py:181
  8.7 228.6 %all-gather.9.cloned.1.call-start = ((), (), s32[]{:S(2)}) async-start(), calls=%async_computation.3 | async-start | bytes 3538944 | tf_op jit(solution)/shard_map/all_gather | solution.py:165
  9.3 253.6 %reduce-scatter.2.cloned.1.call-start = ((), (), s32[]{:S(2)}) async-start(), calls=%async_computation.5 | async-start | bytes 655360 | tf_op jit(solution)/shard_map/reduce_scatter | solution.py:184
  54.9 7.4 %copy-start.1 = (bf16[128,2048]{1,0:T(8,128)(2,1)S(1)}, bf16[128,2048]{1,0:T(8,128)(2,1)}, u32[]{:S(2)}) copy-start(bf16[128,2048]{1,0:T(8,128)(2,1)} %param.15) | copy-start | bytes 1572868
  62.4 57.8 %copy-start.3 = (bf16[3,768]{1,0:T(4,128)(2,1)S(1)}, bf16[3,768]{1,0:T(4,128)(2,1)}, u32[]{:S(2)}) copy-start(bf16[3,768]{1,0:T(4,128)(2,1)} %param.20) | copy-start | bytes 13828
  116.4 121.0 %collective-permute-start = (bf16[1,768]{1,0:T(2,128)(2,1)S(1)}, bf16[1,768]{1,0:T(2,128)(2,1)S(1)}, u32[]{:S(2)}, u32[]{:S(2)}) collective-permute-start(bf16[1,768]{1,0:T(2,128)(2,1)S(1)} %get-tuple-element.8), channel_id=1, source_target_pairs={{0,4},{4,8},{8,12},{12,16},{16,20},{20,24},{24,28},{1,5},{5,9},{9,... | collective-permute-start | bytes 4616 | tf_op jit(solution)/shard_map/ppermute | solution.py:18
  118.8 118.5 %collective-permute-start.1 = (bf16[1,768]{1,0:T(2,128)(2,1)S(1)}, bf16[1,768]{1,0:T(2,128)(2,1)S(1)}, u32[]{:S(2)}, u32[]{:S(2)}) collective-permute-start(bf16[1,768]{1,0:T(2,128)(2,1)S(1)} %get-tuple-element.9), channel_id=1, source_target_pairs={{4,0},{8,4},{12,8},{16,12},{20,16},{24,20},{28,24},{5,1},{9,5},{13... | collective-permute-start | bytes 4616 | tf_op jit(solution)/shard_map/ppermute | solution.py:21
Sparse Core Ops, SparseCore 0:
  9.5 43.2 all-gather.4
  54.9 58.7 all-gather.6
  115.7 61.2 all-gather.10
  179.1 58.1 all-gather.8
  242.6 20.2 reduce-scatter.1
where the time goes:
time: 271 us
  waiting for transfers between devices  204 us (75%)
  blocking collectives  33.8 us (12%)
  between operations  13.3 us (5%)
  matrix products  12.8 us (5%)
  starting transfers between devices  3.9 us (1%)
  other arithmetic  3.68 us (1%)
    all_gather x1, waiting for transfers between devices, body(): lax.all_gather(value_weight, 'sp', axis=0, tiled=True)  60.3 us
    all_gather x1, waiting for transfers between devices, body(): lax.all_gather(down_weight, 'sp', axis=1, tiled=True)  56.9 us
    all_gather x1, waiting for transfers between devices, body(): lax.all_gather(gate_weight, 'sp', axis=0, tiled=True)  49.9 us
    all_gather x1, blocking collectives, body(): lax.all_gather(key_turned, 'sp', axis=0, tiled=True)  28.2 us
    reduce_scatter x1, waiting for transfers between devices, body(): lax.psum_scatter(partial_rows.astype(jnp.bfloat16), 'tp', scatter_dimensi...  20.5 us
    all_gather x1, waiting for transfers between devices, body(): lax.all_gather(latents, 'sp', axis=0, tiled=True)  13.5 us
    all_gather x1, blocking collectives, body(): all_heads = lax.all_gather(attended, 'tp', axis=1, tiled=True)  5.6 us
  transfers between devices with their start and end apart: 7, of which 5 were waited for; matrix products, arithmetic and copies ran while one was open for 4% of the time, Pallas kernels for 0%

commit v1 on v0

--- a/solution.py
+++ b/solution.py
@@ -161,7 +161,9 @@
     normed = normalize(stream, norm_gain)
     stream_own = lax.dynamic_slice_in_dim(stream, tp_index * share, share, 0)
     pieces = (
-        lax.all_gather(gate_weight, "sp", axis=0, tiled=True),
+        jnp.concatenate(
+            lax.all_to_all(jnp.stack([gate_weight] * lax.axis_size("sp")), "sp", 0, 0), axis=0
+        ),
         lax.all_gather(value_weight, "sp", axis=0, tiled=True),
     )
     gate_sum = jnp.dot(normed, pieces[0], preferred_element_type=jnp.float32)

time: 271 us -> 259 us (0.956)
  waiting for transfers between devices: 204 us -> 110 us
  blocking collectives: 33.8 us -> 107 us
  starting transfers between devices: 3.9 us -> 10.1 us
  local copies, waits for them, and re-layouts: 0.03 us -> 2.87 us
    all_gather x1, blocking collectives: 28.2 us -> 102 us  [body(): lax.all_gather(key_turned, 'sp', axis=0, tiled=True)]
    all_gather x1 -> x0, waiting for transfers between devices: 49.9 us -> none  [body(): lax.all_gather(gate_weight, 'sp', axis=0, tiled=True)]
    all_gather x1, waiting for transfers between devices: 60.3 us -> 24.7 us  [body(): lax.all_gather(value_weight, 'sp', axis=0, tiled=True)]
    all_gather x1, waiting for transfers between devices: 13.5 us -> 0.01 us  [body(): lax.all_gather(latents, 'sp', axis=0, tiled=True)]
    all_to_all x0 -> x1, starting transfers between devices: none -> 7.44 us  [body(): lax.all_to_all(jnp.stack([gate_weight] * lax.axis_size('sp')), 'sp', 0, 0)]
    all_gather x1, waiting for transfers between devices: 56.9 us -> 63.4 us  [body(): lax.all_gather(down_weight, 'sp', axis=1, tiled=True)]
    another operation x0 -> x1, local copies, waits for them, and re-layouts: none -> 2.84 us  [body(): jnp.stack([gate_weight] * lax.axis_size('sp'))]
  transfers between devices with their start and end apart: 7 -> 7, of which waited for: 5 -> 3; matrix products, arithmetic and copies ran while one was open for 4% -> 4% of each run, Pallas kernels for 0% -> 0%
where the time goes in v1:
time: 259 us
  waiting for transfers between devices  110 us (42%)
  blocking collectives  107 us (41%)
  between operations  13.3 us (5%)
  matrix products  12.9 us (5%)
  starting transfers between devices  10.1 us (4%)
  local copies, waits for them, and re-layouts  2.87 us (1%)
    all_gather x1, blocking collectives, body(): lax.all_gather(key_turned, 'sp', axis=0, tiled=True)  102 us
    all_gather x1, waiting for transfers between devices, body(): lax.all_gather(down_weight, 'sp', axis=1, tiled=True)  63.4 us
    all_gather x1, waiting for transfers between devices, body(): lax.all_gather(value_weight, 'sp', axis=0, tiled=True)  24.7 us
    reduce_scatter x1, waiting for transfers between devices, body(): lax.psum_scatter(partial_rows.astype(jnp.bfloat16), 'tp', scatter_dimensi...  20 us
    all_to_all x1, starting transfers between devices, body(): lax.all_to_all(jnp.stack([gate_weight] * lax.axis_size('sp')), 'sp', 0, 0)  7.44 us
    all_gather x1, blocking collectives, body(): all_heads = lax.all_gather(attended, 'tp', axis=1, tiled=True)  5.6 us
  transfers between devices with their start and end apart: 7, of which 3 were waited for; matrix products, arithmetic and copies ran while one was open for 4% of the time, Pallas kernels for 0%

profile of v1, /device:TPU:0, one launch (start us, length us, event | category | flops | bytes accessed | tf_op | source)
XLA Modules:
  0.0 259.0 jit_solution(6528066936536387348)
XLA Ops:
  6.5 0.7 all-gather.4.cloned.1.call-update
  7.3 0.0 all-gather.6.cloned.1.call-start
  7.3 0.7 all-gather.6.cloned.1.call-update
  8.0 2.8 %stack.2 = bf16[8,256,768]{2,1,0:T(8,128)(2,1)} broadcast(bf16[256,768]{1,0:T(8,128)(2,1)} %param.18), dimensions={1,2} | broadcast | bytes 3538944 | tf_op jit(solution)/shard_map/stack | solution.py:165
  10.9 7.4 %all-to-all-start = ((bf16[8,256,768]{2,1,0:T(8,128)(2,1)}), bf16[8,256,768]{2,1,0:T(8,128)(2,1)}, u32[]{:S(2)}, u32[]{:S(2)}) async-start(bf16[8,256,768]{2,1,0:T(8,128)(2,1)} %stack.2), calls=%async_computation | async-start | bytes 6291456 | tf_op jit(solution)/shard_map/all_to_all | solution.py:165
  18.3 0.0 all-gather.8.cloned.1.call-start
  18.3 0.7 all-gather.8.cloned.1.call-update
  19.0 0.0 reduce-scatter.2.cloned.1.call-start
  19.1 0.2 fusion.59
  19.3 101.8 %all_gather.16 = bf16[1024,64]{0,1:T(8,128)(2,1)S(1)} all-gather(bf16[128,64]{0,1:T(8,128)(2,1)S(1)} %pad_maximum_fusion.5), channel_id=1, replica_groups=mesh['sp'=8,'tp'=4] {'sp'}, dimensions={0}, use_global_device_ids=true | all-gather | bytes 147456 | tf_op jit(solution)/shard_map/all_gather | solution.py:111
  121.1 1.9 convolution_convert_fusion.1
  123.1 0.3 convolution_bitcast_fusion.1
  123.3 0.0 copy-start.1
  123.3 0.4 fusion.83
  123.7 0.2 fusion.11
  123.9 0.3 convolution_bitcast_fusion
  124.1 0.4 fusion.82
  124.5 0.2 fusion.13
  124.6 0.2 fusion.7
  124.9 0.3 fusion.6
  125.2 5.6 %all_gather.17 = bf16[128,768]{0,1:T(8,128)(2,1)S(1)} all-gather(bf16[128,192]{0,1:T(8,128)(2,1)S(1)} %pad_maximum_fusion.4), channel_id=1, replica_groups=mesh['sp'=8,'tp'=4] {'tp'}, dimensions={1}, use_global_device_ids=true | all-gather | bytes 245760 | tf_op jit(solution)/shard_map/all_gather | solution.py:158
  130.8 1.5 fusion.8
  132.2 2.7 %convolution_convert_fusion.3 = bf16[128,768]{1,0:T(8,128)(2,1)S(1)} fusion(bf16[2048,768]{1,0:T(8,128)(2,1)} %bitcast.2, bf16[128,2048]{1,0:T(8,128)(2,1)} %get-tuple-element.23, f32[2048]{0:T(1024)S(1)} %convert_element_type.113, f32[128]{0:T(128)S(1)} %add_rsqrt_fusion), kind=kOutput, calls=%fused_computation.16 | convolution fusion | flops 403800064 | bytes 3875328 | tf_op jit(solution)/shard_map/dot_general | solution.py:169
  134.9 1.3 collective-permute-start
  136.2 1.3 collective-permute-start.1
  137.6 24.7 %all-gather.6.cloned.1.call-done = bf16[2048,768]{1,0:T(8,128)(2,1)} async-done(((bf16[256,768]{1,0:T(8,128)(2,1)}), bf16[2048,768]{1,0:T(8,128)(2,1)}) %all-gather.6.cloned.1.call-update) | async-done | bytes 3145744 | tf_op jit(solution)/shard_map/all_gather | solution.py:167
  162.3 63.4 %all-gather.8.cloned.1.call-done = bf16[768,2048]{1,0:T(8,128)(2,1)} async-done(((bf16[768,256]{1,0:T(8,128)(2,1)}), bf16[768,2048]{1,0:T(8,128)(2,1)}) %all-gather.8.cloned.1.call-update) | async-done | bytes 3145744 | tf_op jit(solution)/shard_map/all_gather | solution.py:183
  225.7 0.0 collective-permute-done
  225.7 5.1 %convolution_convert_fusion = bf16[128,2048]{1,0:T(8,128)(2,1)} fusion(bf16[768,2048]{1,0:T(8,128)(2,1)} %all-gather.8.cloned.1.call-done, bf16[2048,768]{1,0:T(8,128)(2,1)} %all-gather.6.cloned.1.call-done, bf16[128,768]{1,0:T(8,128)(2,1)S(1)} %convolution_convert_fusion.3, bf16[1,768]{1,0:T(2,128)(2,1)S(1)} %collective-permute-done.1, ...), kind=kOutput, calls=%fused_computation.2 | convolution fusion | flops 808779776 | bytes 7557632 | tf_op jit(solution)/shard_map/dot_general | solution.py:181
  230.8 0.0 reduce-scatter.2.cloned.1.call-update
  230.9 20.0 %reduce-scatter.2.cloned.1.call-done = bf16[32,2048]{1,0:T(8,128)(2,1)} async-done(((bf16[128,2048]{1,0:T(8,128)(2,1)}), bf16[32,2048]{1,0:T(8,128)(2,1)}) %reduce-scatter.2.cloned.1.call-update) | async-done | bytes 131088 | tf_op jit(solution)/shard_map/reduce_scatter | solution.py:186
  250.9 1.7 add_convert_fusion
  (25 shorter events, 0.1 us)
Async XLA Ops:
  6.5 124.2 %copy-start = (bf16[768,2048]{1,0:T(8,128)(2,1)S(1)}, bf16[768,2048]{1,0:T(8,128)(2,1)}, u32[]{:S(2)}) copy-start(bf16[768,2048]{1,0:T(8,128)(2,1)} %param.16) | copy-start | bytes 9437188
  6.5 114.6 %all-gather.4.cloned.1.call-start = ((), (), s32[]{:S(2)}) async-start(), calls=%async_computation.2 | async-start | bytes 1179648 | tf_op jit(solution)/shard_map/all_gather | solution.py:110
  7.3 155.1 %all-gather.6.cloned.1.call-start = ((), (), s32[]{:S(2)}) async-start(), calls=%async_computation.3 | async-start | bytes 3538944 | tf_op jit(solution)/shard_map/all_gather | solution.py:167
  10.8 8.2 %copy-start.5 = (bf16[2048]{0:T(1024)(128)(2,1)S(1)}, bf16[2048]{0:T(1024)(128)(2,1)}, u32[]{:S(2)}) copy-start(bf16[2048]{0:T(1024)(128)(2,1)} %param.17) | copy-start | bytes 12292
  10.8 8.3 %copy-start.2 = (bf16[128,320]{0,1:T(8,128)(2,1)S(1)}, bf16[128,320]{0,1:T(8,128)(2,1)}, u32[]{:S(2)}) copy-start(bf16[128,320]{0,1:T(8,128)(2,1)} %param.11) | copy-start | bytes 245764
  10.9 8.3 %copy-start.3 = (bf16[128,64]{0,1:T(8,128)(2,1)S(1)}, bf16[128,64]{0,1:T(8,128)(2,1)}, u32[]{:S(2)}) copy-start(bf16[128,64]{0,1:T(8,128)(2,1)} %param.13) | copy-start | bytes 49156
  10.9 121.4 %all-to-all-start = ((bf16[8,256,768]{2,1,0:T(8,128)(2,1)}), bf16[8,256,768]{2,1,0:T(8,128)(2,1)}, u32[]{:S(2)}, u32[]{:S(2)}) async-start(bf16[8,256,768]{2,1,0:T(8,128)(2,1)} %stack.2), calls=%async_computation | async-start | bytes 6291456 | tf_op jit(solution)/shard_map/all_to_all | solution.py:165
  18.3 207.4 %all-gather.8.cloned.1.call-start = ((), (), s32[]{:S(2)}) async-start(), calls=%async_computation.4 | async-start | bytes 3538944 | tf_op jit(solution)/shard_map/all_gather | solution.py:183
  19.0 231.8 %reduce-scatter.2.cloned.1.call-start = ((), (), s32[]{:S(2)}) async-start(), calls=%async_computation.5 | async-start | bytes 655360 | tf_op jit(solution)/shard_map/reduce_scatter | solution.py:186
  123.3 7.4 %copy-start.1 = (bf16[128,2048]{1,0:T(8,128)(2,1)S(1)}, bf16[128,2048]{1,0:T(8,128)(2,1)}, u32[]{:S(2)}) copy-start(bf16[128,2048]{1,0:T(8,128)(2,1)} %param.15) | copy-start | bytes 1572868
  130.8 6.8 %copy-start.4 = (bf16[3,768]{1,0:T(4,128)(2,1)S(1)}, bf16[3,768]{1,0:T(4,128)(2,1)}, u32[]{:S(2)}) copy-start(bf16[3,768]{1,0:T(4,128)(2,1)} %param.20) | copy-start | bytes 13828
  134.9 90.8 %collective-permute-start = (bf16[1,768]{1,0:T(2,128)(2,1)S(1)}, bf16[1,768]{1,0:T(2,128)(2,1)S(1)}, u32[]{:S(2)}, u32[]{:S(2)}) collective-permute-start(bf16[1,768]{1,0:T(2,128)(2,1)S(1)} %get-tuple-element.8), channel_id=1, source_target_pairs={{0,4},{4,8},{8,12},{12,16},{16,20},{20,24},{24,28},{1,5},{5,9},{9,... | collective-permute-start | bytes 4616 | tf_op jit(solution)/shard_map/ppermute | solution.py:18
  136.2 89.5 %collective-permute-start.1 = (bf16[1,768]{1,0:T(2,128)(2,1)S(1)}, bf16[1,768]{1,0:T(2,128)(2,1)S(1)}, u32[]{:S(2)}, u32[]{:S(2)}) collective-permute-start(bf16[1,768]{1,0:T(2,128)(2,1)S(1)} %get-tuple-element.9), channel_id=1, source_target_pairs={{4,0},{8,4},{12,8},{16,12},{20,16},{24,20},{28,24},{5,1},{9,5},{13... | collective-permute-start | bytes 4616 | tf_op jit(solution)/shard_map/ppermute | solution.py:21
Sparse Core Ops, SparseCore 0:
  9.5 92.8 all-gather.3
  104.5 57.7 all-gather.5
  164.4 61.3 all-gather.7
  231.0 19.8 reduce-scatter.1
